TPU v7x, 32 devices: a whole 2x2x4 slice. The times are simulated.
32 devices in a mesh: dp: 2 (over x), kv: 8 (over z, y), tp: 2 (over core).
Axes of the slice: x: 2, y: 2, z: 4, core: 2. Of those that a mesh axis runs over, the one named last changes fastest.
Arguments:
- tokens: bfloat16 [32, 3072], P(('tp', 'dp'), 'kv'), parts along dimension 0, may hold values from -60 to 60
- old_state: float32 [32, 24, 128, 128], P(('tp', 'dp', 'kv')), parts along dimension 0, may hold values from -0.6 to 0.6
- mixer_gain: float32 [3072], replicated, may hold values from 0.1 to 1.9
- w_query: bfloat16 [3072, 3072], P(None, 'kv'), may hold values from -0.109375 to 0.109375
- w_key: bfloat16 [3072, 3072], P(None, 'kv'), may hold values from -0.109375 to 0.109375
- w_value: bfloat16 [3072, 3072], P(None, 'kv'), may hold values from -0.109375 to 0.109375
- w_outgate: bfloat16 [3072, 3072], P(None, 'kv'), may hold values from -0.109375 to 0.109375
- w_decay: bfloat16 [3072, 24], replicated, may hold values from -0.109375 to 0.109375
- w_write: bfloat16 [3072, 24], replicated, may hold values from -0.109375 to 0.109375
- decay_log: float32 [24], replicated, may hold values from -3 to 1
- decay_bias: float32 [24], replicated, may hold values from -3 to 3
- head_gain: float32 [128], replicated, may hold values from 0.1 to 1.9
- w_output: bfloat16 [3072, 3072], P('kv'), may hold values from -0.15625 to 0.15625
- channel_gain: float32 [3072], replicated, may hold values from 0.1 to 1.9
- w_gate: bfloat16 [3072, 8448], P(None, 'kv'), may hold values from -0.109375 to 0.109375
- w_up: bfloat16 [3072, 8448], P(None, 'kv'), may hold values from -0.109375 to 0.109375
- w_down: bfloat16 [8448, 3072], P(None, 'kv'), may hold values from -0.0625 to 0.0625
Outputs:
- mixed: bfloat16 [32, 3072], P(('tp', 'dp'), 'kv'), parts along dimension 0
- new_state: float32 [32, 24, 128, 128], P(('tp', 'dp', 'kv')), parts along dimension 0
There are 2 independent parts, one for each index of `tp`. A program takes and returns all parts, laid end to end along the dimension named above; an argument that names none is the same for every part. Nothing has to cross between parts.
All inputs are finite; a program needn't handle non-finite values.
Results may differ from a plain program's by a relative error of at most 0.0059.
Values may be sent and summed in bfloat16 or wider, within the bound.
A program may use at most 64 MiB of HBM per device.

v0:
```python
import jax
import jax.numpy as jnp
from jax import lax
from jax.sharding import PartitionSpec as P

HEADS = 24
HEAD_DIM = 128
EPS = 1e-06


def norm_scale(values):
    return lax.rsqrt(jnp.mean(values * values, axis=-1, keepdims=True) + EPS)


def unit_rows(values):
    return values * lax.rsqrt(jnp.sum(values * values, axis=-1, keepdims=True) + EPS)


def body(
    tokens,
    old_state,
    mixer_gain,
    w_query,
    w_key,
    w_value,
    w_outgate,
    w_decay,
    w_write,
    decay_log,
    decay_bias,
    head_gain,
    w_output,
    channel_gain,
    w_gate,
    w_up,
    w_down,
):
    local_rows = old_state.shape[0]
    width_share = tokens.shape[1]
    offset_rows = lax.axis_index("kv") * local_rows
    offset_cols = lax.axis_index("kv") * width_share
    complete_rows = lax.all_gather(tokens, "kv", axis=1, tiled=True)
    tok_wide = complete_rows.astype(jnp.float32)
    scale_in = norm_scale(tok_wide)
    normed = (tok_wide * mixer_gain).astype(jnp.bfloat16)

    def project(weight):
        return (jnp.dot(normed, weight, preferred_element_type=jnp.float32) * scale_in).astype(
            jnp.bfloat16
        )

    query_cols = project(w_query)
    key_cols = project(w_key)
    value_cols = project(w_value)
    outgate_cols = project(w_outgate)
    query_pre, key_pre, value_pre, outgate_pre = (
        lax.all_to_all(query_cols, "kv", split_axis=0, concat_axis=1, tiled=True),
        lax.all_to_all(key_cols, "kv", split_axis=0, concat_axis=1, tiled=True),
        lax.all_to_all(value_cols, "kv", split_axis=0, concat_axis=1, tiled=True),
        lax.all_to_all(outgate_cols, "kv", split_axis=0, concat_axis=1, tiled=True),
    )
    own_normed = lax.dynamic_slice_in_dim(normed, offset_rows, local_rows, 0)
    own_scale = lax.dynamic_slice_in_dim(scale_in, offset_rows, local_rows, 0)
    decay_pre = jnp.dot(own_normed, w_decay, preferred_element_type=jnp.float32) * own_scale
    write_pre = jnp.dot(own_normed, w_write, preferred_element_type=jnp.float32) * own_scale

    def by_head(values):
        return values.astype(jnp.float32).reshape(local_rows, HEADS, HEAD_DIM)

    queries = unit_rows(jax.nn.silu(by_head(query_pre))) * HEAD_DIM ** (-0.5)
    keys_unit = unit_rows(jax.nn.silu(by_head(key_pre)))
    values_act = jax.nn.silu(by_head(value_pre))
    strength = jax.nn.sigmoid(write_pre)
    retain = jnp.exp(-jnp.exp(decay_log) * jax.nn.softplus(decay_pre + decay_bias))
    recalled_values = jnp.einsum(
        "bhkv,bhk->bhv", old_state, keys_unit, precision=lax.Precision.HIGHEST
    )
    correction = values_act - retain[..., None] * recalled_values
    new_state = (
        retain[..., None, None] * old_state
        + (strength[..., None] * keys_unit)[..., :, None] * correction[..., None, :]
    )
    state_readout = jnp.einsum("bhkv,bhk->bhv", new_state, queries, precision=lax.Precision.HIGHEST)
    gated_read = (
        state_readout * norm_scale(state_readout) * head_gain * jax.nn.silu(by_head(outgate_pre))
    )
    gated_read = gated_read.reshape(local_rows, HEADS * HEAD_DIM).astype(jnp.bfloat16)
    read_cols = lax.all_to_all(gated_read, "kv", split_axis=1, concat_axis=0, tiled=True)
    partial_out = jnp.dot(read_cols, w_output, preferred_element_type=jnp.float32)
    mixer_out = lax.psum(partial_out, "kv")
    residual = lax.optimization_barrier((tok_wide + mixer_out).astype(jnp.bfloat16))
    residual_wide = residual.astype(jnp.float32)
    scale_mid = norm_scale(residual_wide)
    normed_mid = (residual_wide * channel_gain).astype(jnp.bfloat16)
    gate_act = jnp.dot(normed_mid, w_gate, preferred_element_type=jnp.float32) * scale_mid
    upward = jnp.dot(normed_mid, w_up, preferred_element_type=jnp.float32) * scale_mid
    own_residual = lax.dynamic_slice_in_dim(residual_wide, offset_cols, width_share, 1)
    hidden_units = (jax.nn.silu(gate_act) * upward).astype(jnp.bfloat16)
    down_sum = jnp.dot(
        lax.all_gather(hidden_units, "kv", axis=1, tiled=True),
        w_down,
        preferred_element_type=jnp.float32,
    )
    mixed = (own_residual + down_sum).astype(jnp.bfloat16)
    return (mixed, new_state)


def solution(mesh):
    in_specs = (
        P(("tp", "dp"), "kv"),
        P(("tp", "dp", "kv"), None, None, None),
        P(),
        P(None, "kv"),
        P(None, "kv"),
        P(None, "kv"),
        P(None, "kv"),
        P(),
        P(),
        P(),
        P(),
        P(),
        P("kv", None),
        P(),
        P(None, "kv"),
        P(None, "kv"),
        P(None, "kv"),
    )
    out_specs = (P(("tp", "dp"), "kv"), P(("tp", "dp", "kv"), None, None, None))
    return jax.shard_map(body, mesh=mesh, in_specs=in_specs, out_specs=out_specs, check_vma=False)
```

profile of v0, /device:TPU:0, one launch (start us, length us, event | category | flops | bytes accessed | tf_op | source)
XLA Modules:
  0.0 226.5 jit_solution(14168076446692269067)
XLA Ops:
  7.2 32.9 %all_gather.6 = bf16[8,3072]{1,0:T(8,128)(2,1)S(1)} all-gather(bf16[8,384]{1,0:T(8,128)(2,1)} %param.17), channel_id=1, replica_groups=mesh['dp'=2,'kv'=8,'tp'=2] {'kv'}, dimensions={1}, use_global_device_ids=true | all-gather | bytes 55296 | tf_op jit(solution)/shard_map/all_gather | solution.py:42
  40.1 0.8 fusion.24
  41.0 2.1 fusion.15
  44.9 5.4 %all-to-all-start = ((bf16[8,2,192]{2,1,0:T(2,128)(2,1)}), bf16[8,2,192]{2,1,0:T(2,128)(2,1)S(1)}, u32[]{:S(2)}, u32[]{:S(2)}) async-start(bf16[8,2,192]{2,1,0:T(2,128)(2,1)} %reshape.400), calls=%async_computation | async-start | bytes 16384 | tf_op jit(solution)/shard_map/all_to_all | solution.py:58
  50.9 2.2 fusion.14
  54.1 0.8 fusion.46
  54.9 0.8 fusion.20
  59.8 6.0 %all-to-all-start.1 = ((bf16[8,2,192]{2,1,0:T(2,128)(2,1)}), bf16[8,2,192]{2,1,0:T(2,128)(2,1)S(1)}, u32[]{:S(2)}, u32[]{:S(2)}) async-start(bf16[8,2,192]{2,1,0:T(2,128)(2,1)} %reshape.402), calls=%async_computation.1 | async-start | bytes 16384 | tf_op jit(solution)/shard_map/all_to_all | solution.py:59
  66.0 6.3 %all-to-all-done.1 = bf16[8,2,192]{2,1,0:T(2,128)(2,1)S(1)} async-done(((bf16[8,2,192]{2,1,0:T(2,128)(2,1)}), bf16[8,2,192]{2,1,0:T(2,128)(2,1)S(1)}, u32[]{:S(2)}, u32[]{:S(2)}) %all-to-all-start.1) | async-done | bytes 6176 | tf_op jit(solution)/shard_map/all_to_all | solution.py:59
  72.3 3.3 %all-to-all-start.2 = ((bf16[8,2,192]{2,1,0:T(2,128)(2,1)}), bf16[8,2,192]{2,1,0:T(2,128)(2,1)S(1)}, u32[]{:S(2)}, u32[]{:S(2)}) async-start(bf16[8,2,192]{2,1,0:T(2,128)(2,1)} %reshape.398), calls=%async_computation.2 | async-start | bytes 16384 | tf_op jit(solution)/shard_map/all_to_all | solution.py:57
  75.8 6.3 %all-to-all-done.2 = bf16[8,2,192]{2,1,0:T(2,128)(2,1)S(1)} async-done(((bf16[8,2,192]{2,1,0:T(2,128)(2,1)}), bf16[8,2,192]{2,1,0:T(2,128)(2,1)S(1)}, u32[]{:S(2)}, u32[]{:S(2)}) %all-to-all-start.2) | async-done | bytes 6176 | tf_op jit(solution)/shard_map/all_to_all | solution.py:57
  82.1 3.3 %all-to-all-start.3 = ((bf16[8,2,192]{2,1,0:T(2,128)(2,1)}), bf16[8,2,192]{2,1,0:T(2,128)(2,1)S(1)}, u32[]{:S(2)}, u32[]{:S(2)}) async-start(bf16[8,2,192]{2,1,0:T(2,128)(2,1)} %reshape.396), calls=%async_computation.3 | async-start | bytes 16384 | tf_op jit(solution)/shard_map/all_to_all | solution.py:60
  85.8 2.9 %fusion.5 = f32[24,1,128]{2,1,0:T(1,128)S(1)} fusion(f32[24,128,1]{1,2,0:T(1,128)S(1)} %bitcast.127, f32[1,24,128,128]{3,2,1,0:T(8,128)} %param.18), kind=kOutput, calls=%fused_computation.7 | convolution fusion | flops 4718592 | bytes 1597440 | tf_op jit(solution)/shard_map/bhkv,bhk->bhv/dot_general | solution.py:75
  89.5 1.1 copy-done.2
  90.5 1.4 fusion.3
  92.3 0.7 reduce.8
  93.1 12.2 %all_to_all.65 = bf16[8,2,192]{2,1,0:T(2,128)(2,1)S(1)} all-to-all(bf16[8,2,192]{2,1,0:T(2,128)(2,1)S(1)} %reshape.404), channel_id=1, replica_groups=mesh['dp'=2,'kv'=8,'tp'=2] {'kv'}, dimensions={0} | all-to-all | bytes 12288 | tf_op jit(solution)/shard_map/all_to_all | solution.py:88
  105.4 1.1 fusion.40
  106.5 67.6 %all-reduce.2.cloned.1.call-done = f32[8,3072]{1,0:T(8,128)} async-done(((f32[8,3072]{1,0:T(8,128)}), f32[8,3072]{1,0:T(8,128)}) %all-reduce.2.cloned.1.call-update) | async-done | bytes 98320 | tf_op jit(solution)/shard_map/psum | solution.py:90
  174.1 0.9 fusion.25
  175.2 4.6 %convolution_multiply_fusion.1 = f32[8,1056]{1,0:T(8,128)S(1)} fusion(bf16[3072,1056]{0,1:T(8,128)(2,1)} %param.31, f32[3072]{0:T(1024)S(1)} %copy-done.7, bf16[8,3072]{1,0:T(8,128)(2,1)S(1)} %fusion.25, f32[8]{0:T(128)S(1)} %add_rsqrt_fusion), kind=kOutput, calls=%fused_computation.2 | convolution fusion | flops 51986688 | bytes 6583328 | tf_op jit(solution)/shard_map/dot_general | solution.py:95
  179.8 4.6 %fusion.2 = bf16[1,1056,8]{1,2,0:T(8,128)(2,1)S(1)} fusion(bf16[3072,1056]{0,1:T(8,128)(2,1)} %param.32, f32[3072]{0:T(1024)S(1)} %copy-done.7, bf16[8,3072]{1,0:T(8,128)(2,1)S(1)} %fusion.25, f32[8,1056]{1,0:T(8,128)S(1)} %convolution_multiply_fusion.1, f32[8]{0:T(128)S(1)} %add_rsqrt_fusion), kind=kOutput, calls=%fused_computation.4 | convolution fusion | flops 52037376 | bytes 6600224 | tf_op jit(solution)/shard_map/dot_general | solution.py:96
  184.4 30.7 %all-gather = bf16[8,1056,8]{1,2,0:T(8,128)(2,1)S(1)} all-gather(bf16[1,1056,8]{1,2,0:T(8,128)(2,1)S(1)} %fusion.2), channel_id=1, replica_groups=mesh['dp'=2,'kv'=8,'tp'=2] {'kv'}, dimensions={0}, use_global_device_ids=true | all-gather | bytes 152064 | tf_op jit(solution)/shard_map/all_gather | solution.py:100
  215.3 4.4 %fusion.11 = bf16[8,384]{1,0:T(8,128)(2,1)} fusion(bf16[8448,8]{0,1:T(8,128)(2,1)S(1)} %reshape.385, bf16[8448,384]{1,0:T(8,128)(2,1)} %param.33, f32[8,3072]{1,0:T(8,128)S(1)} %convert_element_type.150, s32[]{:T(128)S(6)} %select_n.14), kind=kOutput, calls=%fused_computation.19 | convolution fusion | flops 51910656 | bytes 6641668 | tf_op jit(solution)/shard_map/dot_general | solution.py:99
  (65 shorter events, 9.7 us)
Async XLA Ops:
  7.2 98.2 %copy-start = (bf16[384,3072]{1,0:T(8,128)(2,1)S(1)}, bf16[384,3072]{1,0:T(8,128)(2,1)}, u32[]{:S(2)}) copy-start(bf16[384,3072]{1,0:T(8,128)(2,1)} %param.29) | copy-start | bytes 7077892
  44.9 14.9 %all-to-all-start = ((bf16[8,2,192]{2,1,0:T(2,128)(2,1)}), bf16[8,2,192]{2,1,0:T(2,128)(2,1)S(1)}, u32[]{:S(2)}, u32[]{:S(2)}) async-start(bf16[8,2,192]{2,1,0:T(2,128)(2,1)} %reshape.400), calls=%async_computation | async-start | bytes 16384 | tf_op jit(solution)/shard_map/all_to_all | solution.py:58
  50.3 2.8 %copy-start.3 = (bf16[3072,384]{1,0:T(8,128)(2,1)S(1)}, bf16[3072,384]{1,0:T(8,128)(2,1)}, u32[]{:S(2)}) copy-start(bf16[3072,384]{1,0:T(8,128)(2,1)} %param.20) | copy-start | bytes 7077892
  50.9 2.7 %copy-start.4 = (bf16[3072,384]{1,0:T(8,128)(2,1)S(1)}, bf16[3072,384]{1,0:T(8,128)(2,1)}, u32[]{:S(2)}) copy-start(bf16[3072,384]{1,0:T(8,128)(2,1)} %param.23) | copy-start | bytes 7077892
  53.1 1.0 copy-start.5
  53.1 1.0 copy-start.8
  53.1 1.0 copy-start.9
  53.1 1.8 copy-start.6
  59.8 12.5 %all-to-all-start.1 = ((bf16[8,2,192]{2,1,0:T(2,128)(2,1)}), bf16[8,2,192]{2,1,0:T(2,128)(2,1)S(1)}, u32[]{:S(2)}, u32[]{:S(2)}) async-start(bf16[8,2,192]{2,1,0:T(2,128)(2,1)} %reshape.402), calls=%async_computation.1 | async-start | bytes 16384 | tf_op jit(solution)/shard_map/all_to_all | solution.py:59
  72.3 9.8 %all-to-all-start.2 = ((bf16[8,2,192]{2,1,0:T(2,128)(2,1)}), bf16[8,2,192]{2,1,0:T(2,128)(2,1)S(1)}, u32[]{:S(2)}, u32[]{:S(2)}) async-start(bf16[8,2,192]{2,1,0:T(2,128)(2,1)} %reshape.398), calls=%async_computation.2 | async-start | bytes 16384 | tf_op jit(solution)/shard_map/all_to_all | solution.py:57
  82.1 10.0 %all-to-all-start.3 = ((bf16[8,2,192]{2,1,0:T(2,128)(2,1)}), bf16[8,2,192]{2,1,0:T(2,128)(2,1)S(1)}, u32[]{:S(2)}, u32[]{:S(2)}) async-start(bf16[8,2,192]{2,1,0:T(2,128)(2,1)} %reshape.396), calls=%async_computation.3 | async-start | bytes 16384 | tf_op jit(solution)/shard_map/all_to_all | solution.py:60
  85.4 88.6 %all-reduce.2.cloned.1.call-start = ((), (), s32[]{:S(2)}) async-start(), calls=%async_computation.5 | async-start | bytes 196608 | tf_op jit(solution)/shard_map/psum | solution.py:90
  85.6 3.2 %copy-start.1 = (f32[1,24,128,128]{3,2,1,0:T(8,128)S(1)}, f32[1,24,128,128]{3,2,1,0:T(8,128)}, u32[]{:S(2)}) copy-start(f32[1,24,128,128]{3,2,1,0:T(8,128)} %param.18) | copy-start | bytes 4718596
  88.8 3.4 %copy-start.10 = (f32[128]{0:T(128)S(1)}, f32[128]{0:T(128)}, u32[]{:S(2)}) copy-start(f32[128]{0:T(128)} %param.28) | copy-start | bytes 1540
  89.4 1.1 copy-start.2
  90.5 84.6 %copy-start.7 = (f32[3072]{0:T(1024)S(1)}, f32[3072]{0:T(1024)}, u32[]{:S(2)}) copy-start(f32[3072]{0:T(1024)} %param.30) | copy-start | bytes 36868
Sparse Core Ops, SparseCore 0:
  106.6 67.4 all-reduce.1
where the time goes:
time: 227 us
  waiting for transfers between devices  80.3 us (35%)
  blocking collectives  75.8 us (33%)
  matrix products  25.8 us (11%)
  starting transfers between devices  18.1 us (8%)
  between operations  14.3 us (6%)
  other arithmetic  6.49 us (3%)
  local copies, waits for them, and re-layouts  5.82 us (3%)
    psum x1, waiting for transfers between devices, body(): mixer_out = lax.psum(partial_out, 'kv')  67.6 us
    all_gather x1, blocking collectives, body(): complete_rows = lax.all_gather(tokens, 'kv', axis=1, tiled=True)  32.9 us
    all_gather x1, blocking collectives, body(): lax.all_gather(hidden_units, 'kv', axis=1, tiled=True)  30.7 us
    all_to_all x1, blocking collectives, body(): lax.all_to_all(gated_read, 'kv', split_axis=1, concat_axis=0, tiled=True)  12.2 us
    all_to_all x1, waiting for transfers between devices, body(): lax.all_to_all(query_cols, 'kv', split_axis=0, concat_axis=1, tiled=True)  6.33 us
    all_to_all x1, waiting for transfers between devices, body(): lax.all_to_all(value_cols, 'kv', split_axis=0, concat_axis=1, tiled=True)  6.29 us
    all_to_all x1, starting transfers between devices, body(): lax.all_to_all(value_cols, 'kv', split_axis=0, concat_axis=1, tiled=True)  5.99 us
    all_to_all x1, starting transfers between devices, body(): lax.all_to_all(key_cols, 'kv', split_axis=0, concat_axis=1, tiled=True)  5.36 us
  transfers between devices with their start and end apart: 5, of which 3 were waited for; matrix products, arithmetic and copies ran while one was open for 7% of the time, Pallas kernels for 0%

commit v1 on v0

--- a/solution.py
+++ b/solution.py
@@ -87,7 +87,11 @@
     gated_read = gated_read.reshape(local_rows, HEADS * HEAD_DIM).astype(jnp.bfloat16)
     read_cols = lax.all_to_all(gated_read, "kv", split_axis=1, concat_axis=0, tiled=True)
     partial_out = jnp.dot(read_cols, w_output, preferred_element_type=jnp.float32)
-    mixer_out = lax.psum(partial_out, "kv")
+
+    def pair_slabs(point):
+        return jnp.sum(lax.all_gather(point, "kv"), 0)
+
+    mixer_out = pair_slabs(partial_out)
     residual = lax.optimization_barrier((tok_wide + mixer_out).astype(jnp.bfloat16))
     residual_wide = residual.astype(jnp.float32)
     scale_mid = norm_scale(residual_wide)

time: 227 us -> 181 us (0.80)
  waiting for transfers between devices: 80.3 us -> 25.3 us
  blocking collectives: 75.8 us -> 95.9 us
  between operations: 14.3 us -> 0.91 us
  starting transfers between devices: 18.1 us -> 21.3 us
    psum x1 -> x0, waiting for transfers between devices: 67.6 us -> none  [body(): mixer_out = lax.psum(partial_out, 'kv')]
    all_gather x0 -> x1, blocking collectives: none -> 32.4 us  [pair_slabs(): return jnp.sum(lax.all_gather(point, 'kv'), 0)]
    all_to_all x1 -> x0, blocking collectives: 12.2 us -> none  [body(): lax.all_to_all(gated_read, 'kv', split_axis=1, concat_axis=0, tiled=True)]
    all_to_all x0 -> x1, waiting for transfers between devices: none -> 6.46 us  [body(): lax.all_to_all(gated_read, 'kv', split_axis=1, concat_axis=0, tiled=True)]
    all_to_all x1, waiting for transfers between devices: 0.01 us -> 6.22 us  [body(): lax.all_to_all(outgate_cols, 'kv', split_axis=0, concat_axis=1, tiled=True)]
    all_to_all x0 -> x1, starting transfers between devices: none -> 3.33 us  [body(): lax.all_to_all(gated_read, 'kv', split_axis=1, concat_axis=0, tiled=True)]
    all_to_all x1, starting transfers between devices: 5.99 us -> 3.33 us  [body(): lax.all_to_all(value_cols, 'kv', split_axis=0, concat_axis=1, tiled=True)]
    all_to_all x1, starting transfers between devices: 3.33 us -> 5.99 us  [body(): lax.all_to_all(query_cols, 'kv', split_axis=0, concat_axis=1, tiled=True)]
  transfers between devices with their start and end apart: 5 -> 5, of which waited for: 3 -> 4; matrix products, arithmetic and copies ran while one was open for 7% -> 5% of each run, Pallas kernels for 0% -> 0%
where the time goes in v1:
time: 181 us
  blocking collectives  95.9 us (53%)
  waiting for transfers between devices  25.3 us (14%)
  matrix products  25.1 us (14%)
  starting transfers between devices  21.3 us (12%)
  local copies, waits for them, and re-layouts  6.48 us (4%)
  other arithmetic  5.64 us (3%)
    all_gather x1, blocking collectives, body(): complete_rows = lax.all_gather(tokens, 'kv', axis=1, tiled=True)  32.9 us
    all_gather x1, blocking collectives, pair_slabs(): return jnp.sum(lax.all_gather(point, 'kv'), 0)  32.4 us
    all_gather x1, blocking collectives, body(): lax.all_gather(hidden_units, 'kv', axis=1, tiled=True)  30.6 us
    all_to_all x1, waiting for transfers between devices, body(): lax.all_to_all(gated_read, 'kv', split_axis=1, concat_axis=0, tiled=True)  6.46 us
    all_to_all x1, waiting for transfers between devices, body(): lax.all_to_all(value_cols, 'kv', split_axis=0, concat_axis=1, tiled=True)  6.33 us
    all_to_all x1, waiting for transfers between devices, body(): lax.all_to_all(query_cols, 'kv', split_axis=0, concat_axis=1, tiled=True)  6.28 us
    all_to_all x1, waiting for transfers between devices, body(): lax.all_to_all(outgate_cols, 'kv', split_axis=0, concat_axis=1, tiled=True)  6.22 us
    all_to_all x1, starting transfers between devices, body(): lax.all_to_all(query_cols, 'kv', split_axis=0, concat_axis=1, tiled=True)  5.99 us
  transfers between devices with their start and end apart: 5, of which 4 were waited for; matrix products, arithmetic and copies ran while one was open for 5% of the time, Pallas kernels for 0%

profile of v1, /device:TPU:0, one launch (start us, length us, event | category | flops | bytes accessed | tf_op | source)
XLA Modules:
  0.0 180.7 jit_solution(4412473345242781262)
XLA Ops:
  0.6 32.9 %all_gather.12 = bf16[8,3072]{1,0:T(8,128)(2,1)S(1)} all-gather(bf16[8,384]{1,0:T(8,128)(2,1)} %param.17), channel_id=1, replica_groups=mesh['dp'=2,'kv'=8,'tp'=2] {'kv'}, dimensions={1}, use_global_device_ids=true | all-gather | bytes 55296 | tf_op jit(solution)/shard_map/all_gather | solution.py:42
  33.6 0.8 fusion.24
  34.4 2.1 %fusion.15 = bf16[8,1,384]{2,0,1:T(8,128)(2,1)S(1)} fusion(bf16[8,3072]{1,0:T(8,128)(2,1)S(1)} %get-tuple-element.5, bf16[3072,384]{1,0:T(8,128)(2,1)} %param.21, f32[8]{0:T(128)S(1)} %add_rsqrt_fusion.4), kind=kOutput, calls=%fused_computation.23 | convolution fusion | flops 18880512 | bytes 2414624 | tf_op jit(solution)/shard_map/dot_general | solution.py:48
  38.4 5.4 %all-to-all-start = ((bf16[8,2,192]{2,1,0:T(2,128)(2,1)}), bf16[8,2,192]{2,1,0:T(2,128)(2,1)S(1)}, u32[]{:S(2)}, u32[]{:S(2)}) async-start(bf16[8,2,192]{2,1,0:T(2,128)(2,1)} %reshape.401), calls=%async_computation | async-start | bytes 16384 | tf_op jit(solution)/shard_map/all_to_all | solution.py:58
  44.3 2.2 %fusion.14 = bf16[8,1,384]{2,0,1:T(8,128)(2,1)S(1)} fusion(bf16[8,3072]{1,0:T(8,128)(2,1)S(1)} %get-tuple-element.5, bf16[3072,384]{1,0:T(8,128)(2,1)} %param.22, f32[8]{0:T(128)S(1)} %add_rsqrt_fusion.4), kind=kOutput, calls=%fused_computation.22 | convolution fusion | flops 18880512 | bytes 2414624 | tf_op jit(solution)/shard_map/dot_general | solution.py:48
  47.6 0.8 fusion.46
  48.4 0.8 fusion.20
  53.2 6.0 %all-to-all-start.2 = ((bf16[8,2,192]{2,1,0:T(2,128)(2,1)}), bf16[8,2,192]{2,1,0:T(2,128)(2,1)S(1)}, u32[]{:S(2)}, u32[]{:S(2)}) async-start(bf16[8,2,192]{2,1,0:T(2,128)(2,1)} %reshape.399), calls=%async_computation.2 | async-start | bytes 16384 | tf_op jit(solution)/shard_map/all_to_all | solution.py:57
  59.5 6.3 %all-to-all-done.2 = bf16[8,2,192]{2,1,0:T(2,128)(2,1)S(1)} async-done(((bf16[8,2,192]{2,1,0:T(2,128)(2,1)}), bf16[8,2,192]{2,1,0:T(2,128)(2,1)S(1)}, u32[]{:S(2)}, u32[]{:S(2)}) %all-to-all-start.2) | async-done | bytes 6176 | tf_op jit(solution)/shard_map/all_to_all | solution.py:57
  65.8 3.3 %all-to-all-start.3 = ((bf16[8,2,192]{2,1,0:T(2,128)(2,1)}), bf16[8,2,192]{2,1,0:T(2,128)(2,1)S(1)}, u32[]{:S(2)}, u32[]{:S(2)}) async-start(bf16[8,2,192]{2,1,0:T(2,128)(2,1)} %reshape.397), calls=%async_computation.3 | async-start | bytes 16384 | tf_op jit(solution)/shard_map/all_to_all | solution.py:60
  69.3 6.2 %all-to-all-done.3 = bf16[8,2,192]{2,1,0:T(2,128)(2,1)S(1)} async-done(((bf16[8,2,192]{2,1,0:T(2,128)(2,1)}), bf16[8,2,192]{2,1,0:T(2,128)(2,1)S(1)}, u32[]{:S(2)}, u32[]{:S(2)}) %all-to-all-start.3) | async-done | bytes 6176 | tf_op jit(solution)/shard_map/all_to_all | solution.py:60
  75.6 3.3 %all-to-all-start.1 = ((bf16[8,2,192]{2,1,0:T(2,128)(2,1)}), bf16[8,2,192]{2,1,0:T(2,128)(2,1)S(1)}, u32[]{:S(2)}, u32[]{:S(2)}) async-start(bf16[8,2,192]{2,1,0:T(2,128)(2,1)} %reshape.403), calls=%async_computation.1 | async-start | bytes 16384 | tf_op jit(solution)/shard_map/all_to_all | solution.py:59
  79.0 6.3 %all-to-all-done.1 = bf16[8,2,192]{2,1,0:T(2,128)(2,1)S(1)} async-done(((bf16[8,2,192]{2,1,0:T(2,128)(2,1)}), bf16[8,2,192]{2,1,0:T(2,128)(2,1)S(1)}, u32[]{:S(2)}, u32[]{:S(2)}) %all-to-all-start.1) | async-done | bytes 6176 | tf_op jit(solution)/shard_map/all_to_all | solution.py:59
  85.6 2.9 %fusion.5 = f32[24,1,128]{2,1,0:T(1,128)S(1)} fusion(f32[24,128,1]{1,2,0:T(1,128)S(1)} %bitcast.129, f32[1,24,128,128]{3,2,1,0:T(8,128)} %param.18), kind=kOutput, calls=%fused_computation.7 | convolution fusion | flops 4718592 | bytes 1597440 | tf_op jit(solution)/shard_map/bhkv,bhk->bhv/dot_general | solution.py:75
  89.2 1.1 copy-done.2
  90.3 1.4 fusion.3
  92.0 0.7 reduce.8
  93.4 3.3 %all-to-all-start.4 = ((bf16[8,2,192]{2,1,0:T(2,128)(2,1)}), bf16[8,2,192]{2,1,0:T(2,128)(2,1)S(1)}, u32[]{:S(2)}, u32[]{:S(2)}) async-start(bf16[8,2,192]{2,1,0:T(2,128)(2,1)} %reshape.405), calls=%async_computation.4 | async-start | bytes 16384 | tf_op jit(solution)/shard_map/all_to_all | solution.py:88
  96.7 6.5 %all-to-all-done.4 = bf16[8,2,192]{2,1,0:T(2,128)(2,1)S(1)} async-done(((bf16[8,2,192]{2,1,0:T(2,128)(2,1)}), bf16[8,2,192]{2,1,0:T(2,128)(2,1)S(1)}, u32[]{:S(2)}, u32[]{:S(2)}) %all-to-all-start.4) | async-done | bytes 6176 | tf_op jit(solution)/shard_map/all_to_all | solution.py:88
  103.7 32.4 %all-gather = f32[64,3072]{1,0:T(8,128)S(1)} all-gather(f32[8,3072]{1,0:T(8,128)S(1)} %fusion.40), channel_id=2, replica_groups=mesh['dp'=2,'kv'=8,'tp'=2] {'kv'}, dimensions={0}, use_global_device_ids=true | all-gather | bytes 884736 | tf_op jit(solution)/shard_map/all_gather | solution.py:92
  136.3 4.6 %convolution_multiply_fusion.1 = f32[8,1056]{1,0:T(8,128)S(1)} fusion(bf16[3072,1056]{0,1:T(8,128)(2,1)} %param.31, f32[3072]{0:T(1024)S(1)} %copy-done.7, bf16[8,3072]{1,0:T(8,128)(2,1)S(1)} %fusion.25, f32[8]{0:T(128)S(1)} %add_rsqrt_fusion), kind=kOutput, calls=%fused_computation.2 | convolution fusion | flops 51986688 | bytes 6583328 | tf_op jit(solution)/shard_map/dot_general | solution.py:99
  140.9 4.6 %fusion.2 = bf16[1,1056,8]{1,2,0:T(8,128)(2,1)S(1)} fusion(bf16[3072,1056]{0,1:T(8,128)(2,1)} %param.32, f32[3072]{0:T(1024)S(1)} %copy-done.7, bf16[8,3072]{1,0:T(8,128)(2,1)S(1)} %fusion.25, f32[8,1056]{1,0:T(8,128)S(1)} %convolution_multiply_fusion.1, f32[8]{0:T(128)S(1)} %add_rsqrt_fusion), kind=kOutput, calls=%fused_computation.4 | convolution fusion | flops 52037376 | bytes 6600224 | tf_op jit(solution)/shard_map/dot_general | solution.py:100
  145.6 30.6 %all-gather.1 = bf16[8,1056,8]{1,2,0:T(8,128)(2,1)S(1)} all-gather(bf16[1,1056,8]{1,2,0:T(8,128)(2,1)S(1)} %fusion.2), channel_id=1, replica_groups=mesh['dp'=2,'kv'=8,'tp'=2] {'kv'}, dimensions={0}, use_global_device_ids=true | all-gather | bytes 152064 | tf_op jit(solution)/shard_map/all_gather | solution.py:104
  176.3 4.4 %fusion.11 = bf16[8,384]{1,0:T(8,128)(2,1)} fusion(bf16[8448,8]{0,1:T(8,128)(2,1)S(1)} %reshape.386, bf16[8448,384]{1,0:T(8,128)(2,1)} %param.33, f32[8,3072]{1,0:T(8,128)S(1)} %convert_element_type.150, s32[]{:T(128)S(6)} %select_n.14), kind=kOutput, calls=%fused_computation.19 | convolution fusion | flops 51910656 | bytes 6641668 | tf_op jit(solution)/shard_map/dot_general | solution.py:103
  (65 shorter events, 10.7 us)
Async XLA Ops:
  0.6 102.6 %copy-start = (bf16[384,3072]{1,0:T(8,128)(2,1)S(1)}, bf16[384,3072]{1,0:T(8,128)(2,1)}, u32[]{:S(2)}) copy-start(bf16[384,3072]{1,0:T(8,128)(2,1)} %param.29) | copy-start | bytes 7077892
  38.4 14.9 %all-to-all-start = ((bf16[8,2,192]{2,1,0:T(2,128)(2,1)}), bf16[8,2,192]{2,1,0:T(2,128)(2,1)S(1)}, u32[]{:S(2)}, u32[]{:S(2)}) async-start(bf16[8,2,192]{2,1,0:T(2,128)(2,1)} %reshape.401), calls=%async_computation | async-start | bytes 16384 | tf_op jit(solution)/shard_map/all_to_all | solution.py:58
  43.7 2.8 %copy-start.3 = (bf16[3072,384]{1,0:T(8,128)(2,1)S(1)}, bf16[3072,384]{1,0:T(8,128)(2,1)}, u32[]{:S(2)}) copy-start(bf16[3072,384]{1,0:T(8,128)(2,1)} %param.20) | copy-start | bytes 7077892
  44.3 2.7 %copy-start.4 = (bf16[3072,384]{1,0:T(8,128)(2,1)S(1)}, bf16[3072,384]{1,0:T(8,128)(2,1)}, u32[]{:S(2)}) copy-start(bf16[3072,384]{1,0:T(8,128)(2,1)} %param.23) | copy-start | bytes 7077892
  46.6 1.0 copy-start.5
  46.6 1.0 copy-start.8
  46.6 1.0 copy-start.9
  46.6 1.8 copy-start.6
  53.2 12.5 %all-to-all-start.2 = ((bf16[8,2,192]{2,1,0:T(2,128)(2,1)}), bf16[8,2,192]{2,1,0:T(2,128)(2,1)S(1)}, u32[]{:S(2)}, u32[]{:S(2)}) async-start(bf16[8,2,192]{2,1,0:T(2,128)(2,1)} %reshape.399), calls=%async_computation.2 | async-start | bytes 16384 | tf_op jit(solution)/shard_map/all_to_all | solution.py:57
  65.8 9.8 %all-to-all-start.3 = ((bf16[8,2,192]{2,1,0:T(2,128)(2,1)}), bf16[8,2,192]{2,1,0:T(2,128)(2,1)S(1)}, u32[]{:S(2)}, u32[]{:S(2)}) async-start(bf16[8,2,192]{2,1,0:T(2,128)(2,1)} %reshape.397), calls=%async_computation.3 | async-start | bytes 16384 | tf_op jit(solution)/shard_map/all_to_all | solution.py:60
  75.6 9.8 %all-to-all-start.1 = ((bf16[8,2,192]{2,1,0:T(2,128)(2,1)}), bf16[8,2,192]{2,1,0:T(2,128)(2,1)S(1)}, u32[]{:S(2)}, u32[]{:S(2)}) async-start(bf16[8,2,192]{2,1,0:T(2,128)(2,1)} %reshape.403), calls=%async_computation.1 | async-start | bytes 16384 | tf_op jit(solution)/shard_map/all_to_all | solution.py:59
  85.5 3.1 %copy-start.1 = (f32[1,24,128,128]{3,2,1,0:T(8,128)S(1)}, f32[1,24,128,128]{3,2,1,0:T(8,128)}, u32[]{:S(2)}) copy-start(f32[1,24,128,128]{3,2,1,0:T(8,128)} %param.18) | copy-start | bytes 4718596
  88.6 3.3 %copy-start.10 = (f32[128]{0:T(128)S(1)}, f32[128]{0:T(128)}, u32[]{:S(2)}) copy-start(f32[128]{0:T(128)} %param.28) | copy-start | bytes 1540
  89.2 1.1 copy-start.2
  92.0 44.3 %copy-start.7 = (f32[3072]{0:T(1024)S(1)}, f32[3072]{0:T(1024)}, u32[]{:S(2)}) copy-start(f32[3072]{0:T(1024)} %param.30) | copy-start | bytes 36868
  93.4 9.8 %all-to-all-start.4 = ((bf16[8,2,192]{2,1,0:T(2,128)(2,1)}), bf16[8,2,192]{2,1,0:T(2,128)(2,1)S(1)}, u32[]{:S(2)}, u32[]{:S(2)}) async-start(bf16[8,2,192]{2,1,0:T(2,128)(2,1)} %reshape.405), calls=%async_computation.4 | async-start | bytes 16384 | tf_op jit(solution)/shard_map/all_to_all | solution.py:88
